TPU v7x, 256 devices: a 8x8x2 block of a 8x8x16 slice. The times are simulated.
256 devices in a mesh: grp: 2 (over z), ep: 64 (over y, x), tp: 2 (over core).
Axes of the slice: x: 8, y: 8, z: 2, core: 2. Of those that a mesh axis runs over, the one named last changes fastest.
The devices are a block of a 8x8x16 slice.
Arguments:
- hidden_in: bfloat16 [2048, 2048], P(('grp', 'ep', 'tp')), parts along dimension 0, may hold values from -6 to 6
- query_nope: bfloat16 [2048, 16, 64], P(('grp', 'ep', 'tp')), parts along dimension 0, may hold values from -102 to 102
- query_rope: bfloat16 [2048, 16, 32], P(('grp', 'ep', 'tp')), parts along dimension 0, may hold values from -6 to 6
- new_latent: bfloat16 [2048, 256], P(('grp', 'ep', 'tp')), parts along dimension 0, may hold values from -6 to 6
- new_rope: bfloat16 [2048, 32], P(('grp', 'ep', 'tp')), parts along dimension 0, may hold values from -6 to 6
- cache_latent: bfloat16 [2048, 1024, 256], P(('grp', 'ep', 'tp')), parts along dimension 0, may hold values from -6 to 6
- cache_rope: bfloat16 [2048, 1024, 32], P(('grp', 'ep', 'tp')), parts along dimension 0, may hold values from -6 to 6
- lengths: int32 [2048], P(('grp', 'ep', 'tp')), parts along dimension 0, may hold values from 1 to 1024, as said below
- absorb_key: bfloat16 [256, 16, 64], replicated, may hold values from -0.75 to 0.75
- value_up: bfloat16 [256, 16, 128], replicated, may hold values from -0.375 to 0.375
- out_proj: bfloat16 [2048, 2048], P(None, ('ep', 'tp')), may hold values from -0.125 to 0.125
- gain_mix: bfloat16 [2048], replicated, may hold values from 0.099609375 to 1.8984375
- gain_ffn_in: bfloat16 [2048], replicated, may hold values from 0.099609375 to 1.8984375
- router: bfloat16 [2048, 128], replicated, may hold values from -0.125 to 0.125
- routes: int32 [2048, 6], P(('grp', 'ep')), parts along dimension 0, may hold values from 0 to 127, all different within a row; in each aligned block of 16 rows (0 to 15, 16 to 31, ...) at most 2 rows name the same one
- expert_gate: bfloat16 [128, 2048, 256], P(('ep', 'tp')), may hold values from -0.125 to 0.125
- expert_up: bfloat16 [128, 2048, 256], P(('ep', 'tp')), may hold values from -0.125 to 0.125
- expert_down: bfloat16 [128, 256, 2048], P(('ep', 'tp')), may hold values from -0.375 to 0.375
- shared_gate: bfloat16 [2048, 256], replicated, may hold values from -0.125 to 0.125
- shared_up: bfloat16 [2048, 256], replicated, may hold values from -0.125 to 0.125
- shared_down: bfloat16 [256, 2048], replicated, may hold values from -0.375 to 0.375
- gain_ffn_out: bfloat16 [2048], replicated, may hold values from 0.099609375 to 1.8984375
Outputs:
- layer_out: bfloat16 [2048, 2048], P(('grp', 'ep', 'tp')), parts along dimension 0
There are 2 independent parts, one for each index of `grp`. A program takes and returns all parts, laid end to end along the dimension named above; an argument that names none is the same for every part. Nothing has to cross between parts.
Inputs may be any that keep to these rules, and one draw needn't show every extreme that they name: `lengths`: every sequence holds 1 to 1024 cached positions, and some sequence holds 1024. `routes`: each row names 6 different experts; in each aligned block of 16 rows (the rows of one index of ep) no expert is named by more than 2 rows, and in some block some expert is named by exactly 2 rows.
All inputs are finite; a program needn't handle non-finite values.
Results may differ from a plain program's by a relative error of at most 0.015.
Values may be sent and summed in bfloat16 or wider, within the bound.
A program may use at most 64 MiB of HBM per device.

v0:
```python
import jax
import jax.numpy as jnp
from jax import lax
from jax.sharding import Mesh
from jax.sharding import PartitionSpec as P

ABLK = 512
EP = ("ep_0", "ep_1")
GRP_EP_TP = ("grp", "ep_0", "ep_1", "tp")
EP_TP = ("ep_0", "ep_1", "tp")
GRP_EP = ("grp", "ep_0", "ep_1")


rope_theta = 10000.0
norm_eps = 1e-06
routed_scale = 2.5
masked_score = -1e30


def joined_along(blocks, dim):
    blocks = jnp.moveaxis(blocks, 0, dim)
    dims = blocks.shape
    return blocks.reshape(*dims[:dim], dims[dim] * dims[dim + 1], *dims[dim + 2 :])


def stacked_from(array, axes, sequence):
    blocks = array[None]
    for k in sequence:
        blocks = lax.all_gather(blocks, axes[k], axis=0, tiled=True)
    carried = [lax.axis_size(axes[k]) for k in reversed(sequence)]
    blocks = blocks.reshape(*carried, *array.shape)
    turned = sorted(range(len(sequence)), key=lambda place: sequence[len(sequence) - 1 - place])
    return blocks.transpose(*turned, *range(len(sequence), blocks.ndim)).reshape(-1, *array.shape)


def gathered_by_axis(array, axes, sequence, dim):
    return joined_along(stacked_from(array, axes, sequence), dim)


def split_up(array, dim, count):
    before, after = (array.shape[:dim], array.shape[dim + 1 :])
    return jnp.moveaxis(array.reshape(*before, count, -1, *after), dim, 0)


def sent_and_summed(array, axis, dim):
    count = lax.axis_size(axis)
    blocks = lax.all_to_all(split_up(array, dim, count), axis, 0, 0, tiled=True)
    return jnp.sum(blocks.astype(jnp.float32), axis=0)


def from_everyone(array, axis):
    count = lax.axis_size(axis)
    return lax.all_to_all(
        jnp.broadcast_to(array[None], (count, *array.shape)), axis, 0, 0, tiled=True
    )


def gathered_copies(array, axis, dim):
    blocks = from_everyone(array, axis)
    return joined_along(blocks, dim)


def normalize(values):
    return values * lax.rsqrt(jnp.mean(values * values, axis=-1, keepdims=True) + norm_eps)


def rotate(values, positions):
    half_dim = values.shape[-1] // 2
    inverse = rope_theta ** (-jnp.arange(half_dim, dtype=jnp.float32) * 2.0 / values.shape[-1])
    angles = positions * inverse
    cosine = jnp.cos(angles)
    sine_table = jnp.sin(angles)
    first_half = values[..., :half_dim]
    second_half = values[..., half_dim:]
    return jnp.concatenate(
        [
            first_half * cosine - second_half * sine_table,
            first_half * sine_table + second_half * cosine,
        ],
        axis=-1,
    )


def swiglu(flat_rows, gate_w, up_w, down_w):
    gate_part = jnp.dot(flat_rows, gate_w, preferred_element_type=jnp.float32)
    up_part = jnp.dot(flat_rows, up_w, preferred_element_type=jnp.float32)
    inner_rows = (jax.nn.silu(gate_part) * up_part).astype(jnp.bfloat16)
    return jnp.dot(inner_rows, down_w, preferred_element_type=jnp.float32).astype(jnp.bfloat16)


def local(
    hidden_in,
    query_nope,
    query_rope,
    new_latent,
    new_rope,
    cache_latent,
    cache_rope,
    lengths,
    absorb_key,
    value_up,
    out_proj,
    gain_mix,
    gain_ffn_in,
    router,
    routes,
    expert_gate,
    expert_up,
    expert_down,
    shared_gate,
    shared_up,
    shared_down,
    gain_ffn_out,
):
    seq_count = hidden_in.shape[0]
    positions = lengths.astype(jnp.float32)
    query_latent = jnp.einsum(
        "shn,chn->shc", query_nope, absorb_key, preferred_element_type=jnp.float32
    ).astype(jnp.bfloat16)
    query_pe = rotate(query_rope.astype(jnp.float32), positions[:, None, None]).astype(jnp.bfloat16)
    latent_new = normalize(new_latent.astype(jnp.float32)).astype(jnp.bfloat16)
    key_new = rotate(new_rope.astype(jnp.float32), positions[:, None]).astype(jnp.bfloat16)
    score_scale = (query_nope.shape[-1] + query_rope.shape[-1]) ** (-0.5)
    new_score = (
        jnp.einsum("shc,sc->sh", query_latent, latent_new, preferred_element_type=jnp.float32)
        + jnp.einsum("shr,sr->sh", query_pe, key_new, preferred_element_type=jnp.float32)
    ) * score_scale

    def attend_block(block_index, loop_state):
        running_max, weight_total, weighted_sum = loop_state
        block_start = block_index * ABLK
        block_latent = lax.dynamic_slice_in_dim(cache_latent, block_start, ABLK, 1)
        block_rope = lax.dynamic_slice_in_dim(cache_rope, block_start, ABLK, 1)
        scores = (
            jnp.einsum(
                "shc,skc->shk", query_latent, block_latent, preferred_element_type=jnp.float32
            )
            + jnp.einsum("shr,skr->shk", query_pe, block_rope, preferred_element_type=jnp.float32)
        ) * score_scale
        key_index = block_start + lax.iota(jnp.int32, ABLK)
        in_range = key_index[None, None, :] < lengths[:, None, None]
        scores = jnp.where(in_range, scores, masked_score)
        new_max = jnp.maximum(running_max, jnp.max(scores, axis=-1))
        rescale = jnp.exp(running_max - new_max)
        weights = jnp.exp(scores - new_max[..., None])
        weight_total = weight_total * rescale + jnp.sum(weights, axis=-1)
        weighted_sum = weighted_sum * rescale[..., None] + jnp.einsum(
            "shk,skc->shc",
            weights.astype(jnp.bfloat16),
            block_latent,
            preferred_element_type=jnp.float32,
        )
        return (new_max, weight_total, weighted_sum)

    longest = jnp.max(lengths)
    block_count = (longest + ABLK - 1) // ABLK
    ones_start = jnp.ones_like(new_score)
    sum_start = ones_start[..., None] * latent_new.astype(jnp.float32)[:, None, :]
    final_max, weight_total, weighted_sum = lax.fori_loop(
        0, block_count, attend_block, (new_score, ones_start, sum_start)
    )
    latent_out = (weighted_sum / weight_total[..., None]).astype(jnp.bfloat16)
    heads_out = (
        jnp.einsum("shc,chv->shv", latent_out, value_up, preferred_element_type=jnp.float32)
        .astype(jnp.bfloat16)
        .reshape(seq_count, -1)
    )
    ep_count = lax.axis_size(EP)
    tp_count = lax.axis_size("tp")
    wide_weight = lax.all_to_all(out_proj, "tp", split_axis=0, concat_axis=1, tiled=True)
    half_heads = lax.all_to_all(heads_out, "tp", split_axis=1, concat_axis=0, tiled=True)
    partial_value = jnp.dot(
        gathered_by_axis(half_heads, EP, (0, 1), 0), wide_weight, preferred_element_type=jnp.float32
    )
    column_count = partial_value.shape[1]
    reorder = partial_value.reshape(ep_count, tp_count, seq_count, column_count).transpose(
        1, 0, 2, 3
    )
    reorder = reorder.reshape(tp_count * ep_count * seq_count, column_count)
    summed = sent_and_summed(reorder.astype(jnp.bfloat16), "tp", 0)
    mixed_rows = lax.all_to_all(
        summed.astype(jnp.bfloat16), EP, split_axis=0, concat_axis=1, tiled=True
    )
    after_mix = (
        hidden_in.astype(jnp.float32)
        + gain_mix.astype(jnp.float32) * normalize(mixed_rows.astype(jnp.float32))
    ).astype(jnp.bfloat16)
    ffn_in = (normalize(after_mix.astype(jnp.float32)) * gain_ffn_in.astype(jnp.float32)).astype(
        jnp.bfloat16
    )
    affinity = jax.nn.sigmoid(jnp.dot(ffn_in, router, preferred_element_type=jnp.float32))
    experts_total = router.shape[1]
    own_start = lax.axis_index("tp") * seq_count
    own_routes = lax.dynamic_slice_in_dim(routes, own_start, seq_count, 0)
    choose = own_routes[..., None] == lax.iota(jnp.int32, experts_total)[None, None, :]
    chosen = jnp.sum(jnp.where(choose, affinity[:, None, :], 0.0), axis=-1)
    route_weights = chosen / jnp.sum(chosen, axis=-1, keepdims=True) * routed_scale
    group_rows, top_count = routes.shape
    capacity = 2 * ((group_rows * top_count + experts_total - 1) // experts_total)
    flat_routes = routes.reshape(-1)
    order_index = lax.iota(jnp.int32, group_rows * top_count)
    same_expert = flat_routes[:, None] == flat_routes[None, :]
    earlier = order_index[None, :] < order_index[:, None]
    slot_number = jnp.sum(jnp.logical_and(same_expert, earlier), axis=1)
    slot_number = slot_number.reshape(group_rows, top_count)
    own_slots = lax.dynamic_slice_in_dim(slot_number, own_start, seq_count, 0)
    slot_index = own_routes * capacity + own_slots
    slots_total = experts_total * capacity
    slot_table = jnp.any(
        slot_index[None, :, :] == lax.iota(jnp.int32, slots_total)[:, None, None], axis=-1
    ).astype(jnp.bfloat16)
    outgoing_terms = jnp.dot(slot_table, ffn_in, preferred_element_type=jnp.float32)
    ep_count = lax.axis_size(EP)
    tp_count = lax.axis_size("tp")
    width = outgoing_terms.shape[1]
    slot_terms = outgoing_terms.reshape(ep_count, tp_count, capacity, width)
    chip_rows = sent_and_summed(slot_terms.astype(jnp.bfloat16), "tp", 1).astype(jnp.bfloat16)
    chip_rows = chip_rows.reshape(ep_count, capacity, width)
    received = lax.all_to_all(chip_rows, EP, split_axis=0, concat_axis=0, tiled=True)
    item_count = received.shape[1]
    outputs = swiglu(
        received.reshape(ep_count * item_count, width), expert_gate[0], expert_up[0], expert_down[0]
    )
    chip_back = lax.all_to_all(
        outputs.reshape(ep_count, item_count, width), EP, split_axis=0, concat_axis=0, tiled=True
    )
    both_cores = gathered_copies(chip_back.reshape(ep_count, 1, capacity, width), "tp", 1)
    returned = both_cores.reshape(experts_total, capacity, width)
    picked = returned.reshape(slots_total, -1)[slot_index]
    routed = jnp.sum(picked.astype(jnp.float32) * route_weights[..., None], axis=1)
    shared = swiglu(ffn_in, shared_gate, shared_up, shared_down)
    combined = routed + shared.astype(jnp.float32)
    return (
        after_mix.astype(jnp.float32) + gain_ffn_out.astype(jnp.float32) * normalize(combined)
    ).astype(jnp.bfloat16)


def solution(mesh):
    torus = Mesh(
        mesh.devices.reshape(mesh.shape["grp"], 8, 8, mesh.shape["tp"]),
        ("grp", "ep_0", "ep_1", "tp"),
    )
    in_specs = (
        P(GRP_EP_TP, None),
        P(GRP_EP_TP, None, None),
        P(GRP_EP_TP, None, None),
        P(GRP_EP_TP, None),
        P(GRP_EP_TP, None),
        P(GRP_EP_TP, None, None),
        P(GRP_EP_TP, None, None),
        P(GRP_EP_TP),
        P(),
        P(),
        P(None, EP_TP),
        P(),
        P(),
        P(),
        P(GRP_EP, None),
        P(EP_TP, None, None),
        P(EP_TP, None, None),
        P(EP_TP, None, None),
        P(),
        P(),
        P(),
        P(),
    )
    out_specs = P(GRP_EP_TP, None)
    return jax.shard_map(local, mesh=torus, in_specs=in_specs, out_specs=out_specs, check_vma=False)
```

profile of v0, /device:TPU:513, one launch (start us, length us, event | category | flops | bytes accessed | tf_op | source)
XLA Modules:
  0.0 222.3 jit_solution(7533666111400621798)
XLA Ops:
  6.6 1.4 fusion.75
  10.1 0.8 fusion.51
  11.7 1.2 fusion.23
  13.6 5.0 %while.14 = (s32[]{:T(128)}, f32[8,16]{1,0:T(8,128)S(1)}, f32[8,16]{1,0:T(8,128)S(1)}, f32[8,16,256]{2,1,0:T(8,128)S(1)}, s32[]{:T(128)}, /*index=5*/s32[8]{0:T(...) while((s32[]{:T(128)}, f32[8,16]{1,0:T(8,128)S(1)}, ...), condition=%wide.region_5.6_spmd, body=%wide.region_2.5_spmd.sunk | while | flops 71897856 | bytes 8245659 | solution.py:159
  13.7 2.4 %fusion.104 = f32[8,512,16]{1,2,0:T(8,128)S(1)} fusion(bf16[8,16,256]{2,1,0:T(8,128)(2,1)S(1)} %get-tuple-element.269, bf16[8,1024,256]{2,1,0:T(8,128)(2,1)} %get-tuple-element.268, s32[]{:T(128)S(6)} %select_n.38), kind=kOutput, calls=%fused_computation.3.clone.1 | convolution fusion | flops 33554432 | bytes 2424836 | tf_op jit(solution)/shard_map/while/body/shc,skc->shk/dot_general | solution.py:135
  16.6 2.0 fusion.107
  19.1 23.8 %all_to_all.73 = bf16[8,2,1024]{2,0,1:T(8,128)(2,1)S(1)} all-to-all(bf16[8,2,1024]{2,0,1:T(8,128)(2,1)S(1)} %bitcast.89), channel_id=1, replica_groups=mesh['grp'=2,'ep_0'=8,'ep_1'=8,'tp'=2] {'tp'}, dimensions={1} | all-to-all | bytes 65536 | tf_op jit(solution)/shard_map/all_to_all | solution.py:171
  42.9 20.8 %all_gather.6 = bf16[8,16,1024]{2,1,0:T(8,128)(2,1)} all-gather(bf16[1,16,1024]{2,1,0:T(8,128)(2,1)S(1)} %bitcast.90), channel_id=1, replica_groups=mesh['grp'=2,'ep_0'=8,'ep_1'=8,'tp'=2] {'ep_0'}, dimensions={0}, use_global_device_ids=true | all-gather | bytes 294912 | tf_op jit(solution)/shard_map/all_gather | solution.py:29
  64.5 9.6 %all-to-all-start.1 = ((bf16[2,1024,16]{1,2,0:T(8,128)(2,1)}), bf16[2,1024,16]{1,2,0:T(8,128)(2,1)S(1)}, u32[]{:S(2)}, u32[]{:S(2)}) async-start(bf16[2,1024,16]{1,2,0:T(8,128)(2,1)} %bitcast.78), calls=%async_computation.1 | async-start | bytes 131072 | tf_op jit(solution)/shard_map/all_to_all | solution.py:170
  74.7 35.6 %all-gather.2.cloned.1.call-done = bf16[64,16,1024]{2,1,0:T(8,128)(2,1)} async-done(((bf16[8,16,1024]{2,1,0:T(8,128)(2,1)}), bf16[64,16,1024]{2,1,0:T(8,128)(2,1)}) %all-gather.2.cloned.1.call-update) | async-done | bytes 2097168 | tf_op jit(solution)/shard_map/all_gather | solution.py:29
  110.2 1.8 copy.103
  112.9 8.3 %all_to_all.74 = bf16[2,512,32]{1,2,0:T(8,128)(2,1)S(1)} all-to-all(bf16[2,512,32]{1,2,0:T(8,128)(2,1)S(1)} %copy.106), channel_id=1, replica_groups=mesh['grp'=2,'ep_0'=8,'ep_1'=8,'tp'=2] {'tp'}, dimensions={0} | all-to-all | bytes 131072 | tf_op jit(solution)/shard_map/all_to_all | solution.py:47
  122.1 11.8 %all-to-all-start.3 = ((bf16[64,2,128]{2,1,0:T(2,128)(2,1)}), bf16[64,2,128]{2,1,0:T(2,128)(2,1)S(1)}, u32[]{:S(2)}, u32[]{:S(2)}) async-start(bf16[64,2,128]{2,1,0:T(2,128)(2,1)} %reshape.230), calls=%async_computation.3 | async-start | bytes 65536 | tf_op jit(solution)/shard_map/all_to_all | solution.py:181
  134.2 9.5 %all-to-all-done.3 = bf16[64,2,128]{2,1,0:T(2,128)(2,1)S(1)} async-done(((bf16[64,2,128]{2,1,0:T(2,128)(2,1)}), bf16[64,2,128]{2,1,0:T(2,128)(2,1)S(1)}, u32[]{:S(2)}, u32[]{:S(2)}) %all-to-all-start.3) | async-done | bytes 32800 | tf_op jit(solution)/shard_map/all_to_all | solution.py:181
  144.9 6.0 %all_to_all.75 = bf16[2,64,1,2,2048]{4,1,3,2,0:T(8,128)(2,1)S(1)} all-to-all(bf16[2,64,1,2,2048]{4,1,3,2,0:T(8,128)(2,1)S(1)} %fusion.18), channel_id=1, replica_groups=mesh['grp'=2,'ep_0'=8,'ep_1'=8,'tp'=2] {'tp'}, dimensions={0} | all-to-all | bytes 2097152 | tf_op jit(solution)/shard_map/all_to_all | solution.py:47
  151.6 22.5 %all_to_all.76 = bf16[64,2,2048]{2,1,0:T(2,128)(2,1)S(1)} all-to-all(bf16[64,2,2048]{2,1,0:T(2,128)(2,1)S(1)} %copy.116), channel_id=1, replica_groups=mesh['grp'=2,'ep_0'=8,'ep_1'=8,'tp'=2] {'ep_0','ep_1'}, dimensions={0} | all-to-all | bytes 1048576 | tf_op jit(solution)/shard_map/all_to_all | solution.py:219
  174.4 1.5 fusion.31
  176.7 1.1 reshape.211
  177.9 7.9 %all-to-all-start.6 = ((bf16[64,2,2048]{2,1,0:T(2,128)(2,1)}), bf16[64,2,2048]{2,1,0:T(2,128)(2,1)S(1)}, u32[]{:S(2)}, u32[]{:S(2)}) async-start(bf16[64,2,2048]{2,1,0:T(2,128)(2,1)} %reshape.211), calls=%async_computation.6 | async-start | bytes 1048576 | tf_op jit(solution)/shard_map/all_to_all | solution.py:224
  185.9 1.3 fusion.27
  187.8 13.3 %all-to-all-done.6 = bf16[64,2,2048]{2,1,0:T(2,128)(2,1)S(1)} async-done(((bf16[64,2,2048]{2,1,0:T(2,128)(2,1)}), bf16[64,2,2048]{2,1,0:T(2,128)(2,1)S(1)}, u32[]{:S(2)}, u32[]{:S(2)}) %all-to-all-start.6) | async-done | bytes 524320 | tf_op jit(solution)/shard_map/all_to_all | solution.py:224
  201.6 8.1 %all_to_all.77 = bf16[2,64,1,2,2048]{4,3,1,2,0:T(2,128)(2,1)S(1)} all-to-all(bf16[2,64,1,2,2048]{4,3,1,2,0:T(2,128)(2,1)S(1)} %broadcast_in_dim.34), channel_id=1, replica_groups=mesh['grp'=2,'ep_0'=8,'ep_1'=8,'tp'=2] {'tp'}, dimensions={0} | all-to-all | bytes 2097152 | tf_op jit(solution)/shard_map/all_to_all | solution.py:53
  209.7 1.2 copy.117
  212.6 2.1 multiply_reduce_fusion.1
  (99 shorter events, 13.7 us)
Async XLA Ops:
  6.5 169.4 %copy-start = (bf16[1,256,2048]{2,1,0:T(8,128)(2,1)S(1)}, bf16[1,256,2048]{2,1,0:T(8,128)(2,1)}, u32[]{:S(2)}) copy-start(bf16[1,256,2048]{2,1,0:T(8,128)(2,1)} %param.41) | copy-start | bytes 3145732
  6.6 103.7 %all-gather.2.cloned.1.call-start = ((), (), s32[]{:S(2)}) async-start(), calls=%async_computation.8 | async-start | bytes 2359296 | tf_op jit(solution)/shard_map/all_gather | solution.py:29
  13.6 5.2 %copy-start.3 = (bf16[256,16,128]{2,1,0:T(8,128)(2,1)S(1)}, bf16[256,16,128]{2,1,0:T(8,128)(2,1)}, u32[]{:S(2)}) copy-start(bf16[256,16,128]{2,1,0:T(8,128)(2,1)} %param.33) | copy-start | bytes 3145732
  13.6 50.2 %copy-start.6 = (bf16[2048,16]{0,1:T(8,128)(2,1)S(1)}, bf16[2048,16]{0,1:T(8,128)(2,1)}, u32[]{:S(2)}) copy-start(bf16[2048,16]{0,1:T(8,128)(2,1)} %param.34) | copy-start | bytes 196612
  13.6 2.4 %copy-start.8 = (s32[8]{0:T(128)S(1)}, s32[8]{0:T(128)}, u32[]{:S(2)}) copy-start(s32[8]{0:T(128)} %get-tuple-element.267) | copy-start | bytes 100 | tf_op jit(solution)/shard_map/while
  13.6 2.5 %copy-start.1 = (bf16[8,1024,32]{1,2,0:T(8,128)(2,1)S(1)}, bf16[8,1024,32]{1,2,0:T(8,128)(2,1)}, u32[]{:S(2)}) copy-start(bf16[8,1024,32]{1,2,0:T(8,128)(2,1)} %get-tuple-element.270) | copy-start | bytes 1572868 | tf_op jit(solution)/shard_map/while
  18.6 55.5 %copy-start.9 = (bf16[2048]{0:T(1024)(128)(2,1)S(1)}, bf16[2048]{0:T(1024)(128)(2,1)}, u32[]{:S(2)}) copy-start(bf16[2048]{0:T(1024)(128)(2,1)} %param.35) | copy-start | bytes 12292
  18.6 55.5 %copy-start.10 = (bf16[2048]{0:T(1024)(128)(2,1)S(1)}, bf16[2048]{0:T(1024)(128)(2,1)}, u32[]{:S(2)}) copy-start(bf16[2048]{0:T(1024)(128)(2,1)} %param.36) | copy-start | bytes 12292
  18.6 55.5 %copy-start.11 = (s32[16,6]{0,1:T(8,128)S(1)}, s32[16,6]{0,1:T(8,128)}, u32[]{:S(2)}) copy-start(s32[16,6]{0,1:T(8,128)} %param.38) | copy-start | bytes 1156
  64.5 47.5 %all-to-all-start.1 = ((bf16[2,1024,16]{1,2,0:T(8,128)(2,1)}), bf16[2,1024,16]{1,2,0:T(8,128)(2,1)S(1)}, u32[]{:S(2)}, u32[]{:S(2)}) async-start(bf16[2,1024,16]{1,2,0:T(8,128)(2,1)} %bitcast.78), calls=%async_computation.1 | async-start | bytes 131072 | tf_op jit(solution)/shard_map/all_to_all | solution.py:170
  112.7 31.5 %copy-start.7 = (bf16[8,2048]{1,0:T(8,128)(2,1)S(1)}, bf16[8,2048]{1,0:T(8,128)(2,1)}, u32[]{:S(2)}) copy-start(bf16[8,2048]{1,0:T(8,128)(2,1)} %param.24) | copy-start | bytes 98308
  122.1 21.6 %all-to-all-start.3 = ((bf16[64,2,128]{2,1,0:T(2,128)(2,1)}), bf16[64,2,128]{2,1,0:T(2,128)(2,1)S(1)}, u32[]{:S(2)}, u32[]{:S(2)}) async-start(bf16[64,2,128]{2,1,0:T(2,128)(2,1)} %reshape.230), calls=%async_computation.3 | async-start | bytes 65536 | tf_op jit(solution)/shard_map/all_to_all | solution.py:181
  151.6 24.3 %copy-start.2 = (bf16[1,2048,256]{2,1,0:T(8,128)(2,1)S(1)}, bf16[1,2048,256]{2,1,0:T(8,128)(2,1)}, u32[]{:S(2)}) copy-start(bf16[1,2048,256]{2,1,0:T(8,128)(2,1)} %param.40) | copy-start | bytes 3145732
  175.9 10.0 %copy-start.12 = (bf16[2048]{0:T(1024)(128)(2,1)S(1)}, bf16[2048]{0:T(1024)(128)(2,1)}, u32[]{:S(2)}) copy-start(bf16[2048]{0:T(1024)(128)(2,1)} %param.45) | copy-start | bytes 12292
  176.7 10.8 %copy-start.4 = (bf16[2048,256]{1,0:T(8,128)(2,1)S(1)}, bf16[2048,256]{1,0:T(8,128)(2,1)}, u32[]{:S(2)}) copy-start(bf16[2048,256]{1,0:T(8,128)(2,1)} %param.42) | copy-start | bytes 3145732
  177.9 23.2 %all-to-all-start.6 = ((bf16[64,2,2048]{2,1,0:T(2,128)(2,1)}), bf16[64,2,2048]{2,1,0:T(2,128)(2,1)S(1)}, u32[]{:S(2)}, u32[]{:S(2)}) async-start(bf16[64,2,2048]{2,1,0:T(2,128)(2,1)} %reshape.211), calls=%async_computation.6 | async-start | bytes 1048576 | tf_op jit(solution)/shard_map/all_to_all | solution.py:224
  211.4 1.2 copy-start.5
Sparse Core Ops, SparseCore 0:
  63.9 46.2 all-gather.1
where the time goes:
time: 224 us; the launch traced here: 222 us
  blocking collectives  89.6 us (40%)
  waiting for transfers between devices  58.4 us (26%)
  starting transfers between devices  29.3 us (13%)
  between operations  14.5 us (6%)
  matrix products  13.5 us (6%)
  local copies, waits for them, and re-layouts  9.69 us (4%)
  other arithmetic  7.24 us (3%)
    all_gather x1, waiting for transfers between devices, stacked_from(): blocks = lax.all_gather(blocks, axes[k], axis=0, tiled=True)  35.6 us
    all_to_all x1, blocking collectives, local(): lax.all_to_all(heads_out, 'tp', split_axis=1, concat_axis=0, tiled=True)  23.8 us
    all_to_all x1, blocking collectives, local(): lax.all_to_all(chip_rows, EP, split_axis=0, concat_axis=0, tiled=True)  22.5 us
    all_gather x1, blocking collectives, stacked_from(): blocks = lax.all_gather(blocks, axes[k], axis=0, tiled=True)  20.8 us
    all_to_all x2, blocking collectives, sent_and_summed(): blocks = lax.all_to_all(split_up(array, dim, count), axis, 0, 0, tiled=True)  14.3 us
    all_to_all x1, waiting for transfers between devices, local(): lax.all_to_all(outputs.reshape(ep_count, item_count, width), EP, split_ax...  13.3 us
    all_to_all x1, starting transfers between devices, local(): lax.all_to_all(summed.astype(jnp.bfloat16), EP, split_axis=0, concat_axis...  11.8 us
    all_to_all x1, starting transfers between devices, local(): lax.all_to_all(out_proj, 'tp', split_axis=0, concat_axis=1, tiled=True)  9.62 us
  transfers between devices with their start and end apart: 4, of which 3 were waited for; matrix products, arithmetic and copies ran while one was open for 2% of the time, Pallas kernels for 0%

commit v1 on v0

v1 whole, which is shorter than its diff:
```python
import functools

import jax
import jax.numpy as jnp
from jax import lax
from jax.experimental import pallas as pl
from jax.experimental.pallas import tpu as pltpu
from jax.sharding import Mesh
from jax.sharding import PartitionSpec as P

MESH = pl.DeviceIdType.MESH
GRP_EP_TP = ("grp", "ep_0", "ep_1", "tp")
EP_TP = ("ep_0", "ep_1", "tp")
GRP_EP = ("grp", "ep_0", "ep_1")

ROPE_THETA = 10000.0
EPS = 1e-06
ROUTED_SCALE = 2.5
MASKED = -1e30
CAP = 2
Q = 4

F32 = jnp.float32
BF16 = jnp.bfloat16
NT = (((1,), (1,)), ((), ()))


def mm(a, b):
    return jnp.dot(a, b, preferred_element_type=F32)


def mm_nt(a, b):
    return lax.dot_general(a, b, NT, preferred_element_type=F32)


def iota(shape, dim):
    return lax.broadcasted_iota(jnp.int32, shape, dim)


def normalize(v):
    return v * lax.rsqrt(jnp.mean(v * v, axis=-1, keepdims=True) + EPS)


def far_first(n):
    return sorted(range(1, n), key=lambda d: (-min(d, n - d), d))


def kernel(
    ny,
    nx,
    lens,
    hid_hbm,
    qn_hbm,
    qr_hbm,
    nl_hbm,
    nr_hbm,
    cl_hbm,
    cr_hbm,
    ak_hbm,
    vu_hbm,
    wt_hbm,
    gmix_hbm,
    gin_hbm,
    gout_hbm,
    router_hbm,
    routes_hbm,
    eg_hbm,
    eu_hbm,
    ed_hbm,
    sg_hbm,
    su_hbm,
    sd_hbm,
    out_ref,
    hid,
    qn,
    qr,
    nl,
    nr,
    cl,
    cr,
    ak,
    vu,
    wtb,
    gmix,
    gin,
    gout,
    router,
    routes,
    eg,
    eu,
    ed,
    sg,
    su,
    sd,
    q32,
    ql,
    lo,
    vut,
    abuf,
    mo,
    mb,
    ffs,
    amx,
    perm,
    permt,
    disp,
    sb,
    rb,
    sb2,
    cb,
    part,
    pb,
    shr,
    lsem,
    csem,
    hsend,
    hrecv,
    wsend,
    wrecv,
    w2send,
    w2recv,
    asend,
    arecv,
    msend,
    mrecv,
    dsend,
    drecv,
    csend,
    crecv,
    psend,
    precv,
):
    y = lax.axis_index("ep_0")
    x = lax.axis_index("ep_1")
    t = lax.axis_index("tp")
    u = 1 - t
    me = y * nx + x
    n_ep = ny * nx
    seqs, heads = qn_hbm.shape[0], qn_hbm.shape[1]
    width = hid_hbm.shape[1]
    qw = width // Q
    experts = router_hbm.shape[1]
    rows_x = n_ep * CAP
    rows_r = n_ep * Q * CAP

    def dev(ty, tx, tt):
        return {"ep_0": ty, "ep_1": tx, "tp": tt}

    def remote(src, dst, ssem, rsem, where):
        return pltpu.make_async_remote_copy(
            src_ref=src, dst_ref=dst, send_sem=ssem, recv_sem=rsem, device_id=dev(*where), device_id_type=MESH
        )

    barrier = pltpu.get_barrier_semaphore()

    def greet(ty, tx, tt):
        pl.semaphore_signal(barrier, inc=1, device_id=dev(ty, tx, tt), device_id_type=MESH)

    def greet_ep(k, _):
        k = lax.rem(me + k, n_ep)
        greet(k // nx, lax.rem(k, nx), t)
        return 0

    greet(y, x, u)
    lax.fori_loop(1, n_ep, greet_ep, 0)
    for d in range(1, ny):
        greet(lax.rem(y + d, ny), x, u)
    peers = 1 + (n_ep - 1) + (ny - 1)

    small = [
        (qn_hbm, qn),
        (ak_hbm, ak),
        (qr_hbm, qr),
        (nl_hbm, nl),
        (nr_hbm, nr),
        (vu_hbm, vu),
        (wt_hbm, wtb.at[x, t]),
        (routes_hbm, routes),
        (hid_hbm, hid.at[t]),
        (gmix_hbm, gmix),
        (gin_hbm, gin),
        (gout_hbm, gout),
        (router_hbm, router),
        (sg_hbm, sg),
        (su_hbm, su),
        (sd_hbm, sd),
        (eg_hbm, eg),
        (eu_hbm, eu),
        (ed_hbm, ed),
    ]
    loads = [pltpu.make_async_copy(a, b, lsem.at[i]) for i, (a, b) in enumerate(small)]
    cache = []
    for s in range(seqs):
        cache.append(
            (
                pltpu.make_async_copy(cl_hbm.at[s], cl.at[s], csem.at[0, s]),
                pltpu.make_async_copy(cr_hbm.at[s], cr.at[s], csem.at[1, s]),
            )
        )
    for i in range(5):
        loads[i].start()
    for a, b in cache:
        a.start()
        b.start()
    for i in range(5, len(loads)):
        loads[i].start()

    loads[0].wait()
    loads[1].wait()
    q32[...] = qn[...].astype(F32)
    for h in range(heads):
        ql[:, h, :] = mm(q32[:, h, :].astype(BF16), ak[h])
    for i in (2, 3, 4):
        loads[i].wait()
    rope = nr.shape[1]
    half = rope // 2
    row8 = iota((seqs, rope), 0)
    pos = jnp.zeros((seqs, rope), F32)
    for s in range(seqs):
        pos = jnp.where(row8 == s, lens[s].astype(F32), pos)
    lane = iota((seqs, rope), 1)
    freq = jnp.exp((lane % half).astype(F32) * (-2.0 / rope * jnp.log(jnp.float32(ROPE_THETA))))
    angle = pos * freq
    cos = jnp.cos(angle)
    sin = jnp.where(lane < half, -jnp.sin(angle), jnp.sin(angle))
    swap = (iota((rope, rope), 0) == (iota((rope, rope), 1) + half) % rope).astype(BF16)
    key_new = (nr[...].astype(F32) * cos + mm(nr[...], swap) * sin).astype(BF16).astype(F32)
    lat_new = normalize(nl[...].astype(F32)).astype(BF16).astype(F32)
    scale = (qn.shape[2] + rope) ** (-0.5)

    ctx = cl.shape[1]
    key_at = iota((heads, ctx), 1)
    for s in range(seqs):
        q_s = ql[s].astype(BF16)
        r_s = qr[s]
        pe_s = (r_s.astype(F32) * cos[s : s + 1, :] + mm(r_s, swap) * sin[s : s + 1, :]).astype(BF16)
        s_new = (
            jnp.sum(q_s.astype(F32) * lat_new[s : s + 1, :], axis=-1, keepdims=True)
            + jnp.sum(pe_s.astype(F32) * key_new[s : s + 1, :], axis=-1, keepdims=True)
        ) * scale
        cache[s][0].wait()
        cache[s][1].wait()
        k_s = cl[s]
        sc = (mm_nt(q_s, k_s) + mm(pe_s, cr[s])) * scale
        sc = jnp.where(key_at < lens[s], sc, MASKED)
        top = jnp.maximum(jnp.max(sc, axis=-1, keepdims=True), s_new)
        p = jnp.exp(sc - top)
        p_new = jnp.exp(s_new - top)
        total = jnp.sum(p, axis=-1, keepdims=True) + p_new
        acc = mm(p.astype(BF16), k_s) + p_new.astype(BF16).astype(F32) * lat_new[s : s + 1, :]
        lo[s] = acc / total

    lat = vut.shape[1]
    pv = (iota((256, 256), 1) == (iota((256, 256), 0) % 16) * heads + iota((256, 256), 0) // 16).astype(BF16)
    loads[5].wait()
    for b in range(lat // 16):
        turned = mm(pv, vu[b * 256 : (b + 1) * 256, :]).astype(BF16)
        vut[:, b * 16 : (b + 1) * 16, :] = turned.reshape(heads, 16, vut.shape[2])
    vh = vut.shape[2]
    for h in range(heads):
        abuf[y, :, h * vh : (h + 1) * vh] = mm(lo[:, h, :].astype(BF16), vut[h]).astype(BF16)

    pl.semaphore_wait(barrier, peers)
    a_out = []
    for d in far_first(ny):
        c = remote(abuf.at[y], abuf.at[y], asend.at[d], arecv.at[d], (lax.rem(y + d, ny), x, t))
        c.start()
        a_out.append(c)
    loads[6].wait()
    w_out = []
    for d in far_first(nx):
        c = remote(wtb.at[x, t], wtb.at[x, t], wsend.at[d], wrecv.at[d], (y, lax.rem(x + d, nx), t))
        c.start()
        w_out.append(c)
    loads[8].wait()
    h_out = remote(hid.at[t], hid.at[t], hsend, hrecv, (y, x, u))
    h_out.start()
    w2_out = [remote(wtb.at[x, t], wtb.at[x, t], w2send.at[0], w2recv.at[0], (y, x, u))]
    w2_out[0].start()

    tokens = 2 * seqs
    loads[7].wait()
    routes_t = routes[...]
    top_k = routes_t.shape[0]
    expert_at = iota((experts, tokens), 0)
    mask = jnp.zeros((experts, tokens), F32)
    for j in range(top_k):
        mask = mask + jnp.where(expert_at == routes_t[j : j + 1, :], 1.0, 0.0)
    before = (iota((tokens, tokens), 0) < iota((tokens, tokens), 1)).astype(BF16)
    place = mm(mask.astype(BF16), before)
    first = jnp.where(place < 0.5, mask, 0.0)
    second = mask - first
    pick = (iota((rows_r, experts), 1) == (iota((rows_r, experts), 0) // (Q * CAP)) * 2 + t).astype(BF16)
    r_q = (iota((rows_r, Q * tokens), 0) // CAP) % Q
    r_cap = iota((rows_r, Q * tokens), 0) % CAP
    c_q = iota((rows_r, Q * tokens), 1) // tokens
    rep = lambda v: jnp.concatenate([v] * Q, axis=1)
    b0 = mm(pick, rep(first).astype(BF16))
    b1 = mm(pick, rep(second).astype(BF16))
    disp[...] = jnp.where(r_q == c_q, jnp.where(r_cap == 0, b0, b1), 0.0).astype(BF16)
    pr, pc = iota((rows_r, rows_r), 0), iota((rows_r, rows_r), 1)
    k = pr % rows_x
    perm[...] = (pc == (k // CAP) * (Q * CAP) + (pr // rows_x) * CAP + k % CAP).astype(BF16)
    k = pc % rows_x
    permt[...] = (pr == (k // CAP) * (Q * CAP) + (pc // rows_x) * CAP + k % CAP).astype(BF16)

    for i, d in enumerate(far_first(nx)[::-1]):
        sx = lax.rem(x + nx - d, nx)
        remote(wtb.at[sx, t], wtb.at[sx, t], wsend.at[d], wrecv.at[d], (y, x, u)).wait_recv()
        c = remote(wtb.at[sx, t], wtb.at[sx, t], w2send.at[d], w2recv.at[d], (y, x, u))
        c.start()
        w2_out.append(c)
    for d in far_first(ny):
        remote(abuf.at[y], abuf.at[y], asend.at[d], arecv.at[d], (y, x, u)).wait_recv()
    for c in w2_out:
        c.wait_recv()
    cols = nx * 2 * wtb.shape[2]
    a_all = abuf[...].reshape(ny * seqs, abuf.shape[2])
    w_all = wtb[...].reshape(cols, wtb.shape[3])
    mo[...] = mm_nt(a_all, w_all).reshape(ny, seqs, cols).astype(BF16)
    m_out = []
    for d in far_first(ny):
        ty = lax.rem(y + d, ny)
        for i, tt in enumerate((t, u)):
            c = remote(mo.at[ty], mb.at[y, t], msend.at[i, d], mrecv.at[i, d], (ty, x, tt))
            c.start()
            m_out.append(c)
    c = remote(mo.at[y], mb.at[y, t], msend.at[1, 0], mrecv.at[1, 0], (y, x, u))
    c.start()
    m_out.append(c)
    mb[y, t] = mo[y]
    for i in range(9, len(loads)):
        loads[i].wait()
    h_out.wait_recv()
    for d in far_first(ny):
        for i in (0, 1):
            remote(mo.at[y], mb.at[y, t], msend.at[i, d], mrecv.at[i, d], (y, x, u)).wait_recv()
    m_out[-1].wait_recv()

    def row_of(g):
        g = g[...].astype(F32)
        return jnp.concatenate([g[i : i + 1, :] for i in range(g.shape[0])], axis=1)

    mixed = jnp.concatenate([mb[i].astype(F32).reshape(tokens, cols) for i in range(ny)], axis=1)
    hidden = hid[...].astype(F32).reshape(tokens, width)
    after = (hidden + row_of(gmix) * normalize(mixed)).astype(BF16).astype(F32)
    ffn = (normalize(after) * row_of(gin)).astype(BF16)
    amx[...] = after.reshape(2, seqs, width)
    ffs[...] = ffn.astype(F32).reshape(2, seqs, width)

    stack = jnp.concatenate([ffn[:, i * qw : (i + 1) * qw] for i in range(Q)], axis=0)
    sb[...] = mm(disp[...], stack).reshape(n_ep, Q * CAP, qw).astype(BF16)
    offsets = sorted(
        [(dy, dx) for dy in range(ny) for dx in range(nx) if (dy, dx) != (0, 0)],
        key=lambda o: (-(min(o[0], ny - o[0]) + min(o[1], nx - o[1])), (o[0] + o[1]) % 2, o),
    )

    def spread(src, dst, ssem, rsem):
        for dy, dx in offsets:
            ty, tx = lax.rem(y + dy, ny), lax.rem(x + dx, nx)
            remote(src.at[ty * nx + tx], dst.at[me], ssem, rsem, (ty, tx, t)).start()
        dst[me] = src[me]

    def arrived(buf, sem):
        some = buf.at[pl.ds(0, n_ep - 1)]
        pltpu.make_async_copy(some, some, sem).wait()

    spread(sb, rb, dsend, drecv)

    own = ffs[t].astype(BF16)
    s_gate = mm(own, sg[...])
    s_up = mm(own, su[...])
    s_hid = (s_gate / (1.0 + jnp.exp(-s_gate)) * s_up).astype(BF16)
    shared = mm(s_hid, sd[...]).astype(BF16).astype(F32)
    shr[...] = jnp.concatenate([shared[:, i * qw : (i + 1) * qw] for i in range(Q)], axis=0)

    logits = lax.dot_general(router[...], ffn, (((0,), (1,)), ((), ())), preferred_element_type=F32)
    aff = mask / (1.0 + jnp.exp(-logits))
    weight = aff * (ROUTED_SCALE / jnp.sum(aff, axis=0, keepdims=True))

    def by_owner(v):
        return jnp.concatenate([v[:, i * seqs : (i + 1) * seqs] for i in (0, 1) for _ in range(Q)], axis=1)

    def to_slots(v):
        return lax.dot_general(v, pick, (((0,), (1,)), ((), ())), preferred_element_type=F32)

    g_q = (iota((Q * tokens, rows_r), 0) // seqs) % Q
    gr_q = (iota((Q * tokens, rows_r), 1) // CAP) % Q
    gr_cap = iota((Q * tokens, rows_r), 1) % CAP

    def combine_of(part_of):
        w0, w1 = part_of(by_owner(weight * first)), part_of(by_owner(weight * second))
        return jnp.where(g_q == gr_q, jnp.where(gr_cap == 0, to_slots(w0), to_slots(w1)), 0.0).astype(BF16)

    g_hi = combine_of(lambda v: v.astype(BF16))
    g_lo = combine_of(lambda v: (v - v.astype(BF16).astype(F32)).astype(BF16))

    arrived(rb, drecv)
    turned = mm(perm[...], rb[...].reshape(rows_r, qw)).astype(BF16)
    gate = jnp.zeros((rows_x, eg.shape[1]), F32)
    up = jnp.zeros((rows_x, eg.shape[1]), F32)
    for i in range(Q):
        piece = turned[i * rows_x : (i + 1) * rows_x, :]
        gate = gate + mm(piece, eg[i * qw : (i + 1) * qw, :])
        up = up + mm(piece, eu[i * qw : (i + 1) * qw, :])
    e_hid = (gate / (1.0 + jnp.exp(-gate)) * up).astype(BF16)
    e_out = jnp.concatenate([mm(e_hid, ed[:, i * qw : (i + 1) * qw]).astype(BF16) for i in range(Q)], axis=0)
    sb2[...] = mm(permt[...], e_out).reshape(n_ep, Q * CAP, qw).astype(BF16)
    spread(sb2, cb, csend, crecv)

    arrived(cb, crecv)
    c_all = cb[...].reshape(rows_r, qw)
    routed = mm(g_hi, c_all) + mm(g_lo, c_all)
    part[...] = routed.reshape(2, Q * seqs, qw)
    p_out = remote(part.at[u], pb, psend, precv, (y, x, u))
    p_out.start()
    mine = part[t] + shr[...]
    after_own = amx[t]
    g_out = row_of(gout)
    p_out.wait_recv()
    comb = mine + pb[...]
    comb = jnp.concatenate([comb[i * seqs : (i + 1) * seqs, :] for i in range(Q)], axis=1)
    out_ref[...] = (after_own + g_out * normalize(comb)).astype(BF16)

    for c in a_out + w_out + w2_out + m_out + [h_out, p_out]:
        c.wait_send()
    arrived(sb, dsend)
    arrived(sb2, csend)


def local(
    ny,
    nx,
    hidden_in,
    query_nope,
    query_rope,
    new_latent,
    new_rope,
    cache_latent,
    cache_rope,
    lengths,
    absorb_key,
    value_up,
    out_proj,
    gain_mix,
    gain_ffn_in,
    router,
    routes,
    expert_gate,
    expert_up,
    expert_down,
    shared_gate,
    shared_up,
    shared_down,
    gain_ffn_out,
):
    seqs, width = hidden_in.shape
    heads = query_nope.shape[1]
    lat, vh = value_up.shape[0], value_up.shape[2]
    feats = heads * vh
    col = out_proj.shape[1]
    n_ep = ny * nx
    qw = width // Q
    experts = router.shape[1]
    rows_r = n_ep * Q * CAP
    tokens = 2 * seqs
    args = (
        lengths,
        hidden_in,
        query_nope,
        query_rope,
        new_latent,
        new_rope,
        cache_latent,
        cache_rope.transpose(0, 2, 1),
        absorb_key.transpose(1, 2, 0),
        value_up.reshape(lat * heads, vh),
        out_proj.T,
        gain_mix.reshape(-1, 128),
        gain_ffn_in.reshape(-1, 128),
        gain_ffn_out.reshape(-1, 128),
        router,
        routes.T,
        expert_gate[0],
        expert_up[0],
        expert_down[0],
        shared_gate,
        shared_up,
        shared_down,
    )
    v = pltpu.VMEM
    dma = pltpu.SemaphoreType.DMA

    def like(i):
        return v(args[i].shape, args[i].dtype)

    scratch = [
        v((2, seqs, width), BF16),
        like(2),
        like(3),
        like(4),
        like(5),
        like(6),
        like(7),
        like(8),
        like(9),
        v((nx, 2, col, feats), BF16),
        like(11),
        like(12),
        like(13),
        like(14),
        like(15),
        like(16),
        like(17),
        like(18),
        like(19),
        like(20),
        like(21),
        v(query_nope.shape, F32),
        v((seqs, heads, lat), F32),
        v((seqs, heads, lat), F32),
        v((heads, lat, vh), BF16),
        v((ny, seqs, feats), BF16),
        v((ny, seqs, nx * 2 * col), BF16),
        v((ny, 2, seqs, nx * 2 * col), BF16),
        v((2, seqs, width), F32),
        v((2, seqs, width), F32),
        v((rows_r, rows_r), BF16),
        v((rows_r, rows_r), BF16),
        v((rows_r, Q * tokens), BF16),
        v((n_ep, Q * CAP, qw), BF16),
        v((n_ep, Q * CAP, qw), BF16),
        v((n_ep, Q * CAP, qw), BF16),
        v((n_ep, Q * CAP, qw), BF16),
        v((2, Q * seqs, qw), F32),
        v((Q * seqs, qw), F32),
        v((Q * seqs, qw), F32),
        dma((19,)),
        dma((2, seqs)),
        dma,
        dma,
        dma((nx,)),
        dma((nx,)),
        dma((nx,)),
        dma((nx,)),
        dma((ny,)),
        dma((ny,)),
        dma((2, ny)),
        dma((2, ny)),
        dma,
        dma,
        dma,
        dma,
        dma,
        dma,
    ]
    hbm = pl.BlockSpec(memory_space=pltpu.HBM)
    return pl.pallas_call(
        functools.partial(kernel, ny, nx),
        out_shape=jax.ShapeDtypeStruct((seqs, width), BF16),
        in_specs=[pl.BlockSpec(memory_space=pltpu.SMEM)] + [hbm] * (len(args) - 1),
        out_specs=pl.BlockSpec(memory_space=pltpu.VMEM),
        scratch_shapes=scratch,
        compiler_params=pltpu.CompilerParams(
            collective_id=0, has_side_effects=True, vmem_limit_bytes=60 * 1024 * 1024
        ),
        name="layer",
    )(*args)


def solution(mesh):
    side = int(round(mesh.shape["ep"] ** 0.5))
    ny, nx = side, mesh.shape["ep"] // side
    torus = Mesh(
        mesh.devices.reshape(mesh.shape["grp"], ny, nx, mesh.shape["tp"]),
        ("grp", "ep_0", "ep_1", "tp"),
    )
    in_specs = (
        P(GRP_EP_TP, None),
        P(GRP_EP_TP, None, None),
        P(GRP_EP_TP, None, None),
        P(GRP_EP_TP, None),
        P(GRP_EP_TP, None),
        P(GRP_EP_TP, None, None),
        P(GRP_EP_TP, None, None),
        P(GRP_EP_TP),
        P(),
        P(),
        P(None, EP_TP),
        P(),
        P(),
        P(),
        P(GRP_EP, None),
        P(EP_TP, None, None),
        P(EP_TP, None, None),
        P(EP_TP, None, None),
        P(),
        P(),
        P(),
        P(),
    )
    return jax.shard_map(
        functools.partial(local, ny, nx),
        mesh=torus,
        in_specs=in_specs,
        out_specs=P(GRP_EP_TP, None),
        check_vma=False,
    )
```

time: 224 us -> 81.4 us (0.36)
  blocking collectives: 89.6 us -> 0 us
  Pallas kernels: 0 us -> 79.9 us
  waiting for transfers between devices: 58.4 us -> 0 us
  starting transfers between devices: 29.3 us -> 0 us
  between operations: 14.5 us -> 0.01 us
  matrix products: 13.5 us -> 0 us
  local copies, waits for them, and re-layouts: 9.69 us -> 1.38 us
  other arithmetic: 7.24 us -> 0 us
    pallas_call x0 -> x1, Pallas kernels: none -> 79.9 us  [local(): pl.pallas_call(functools.partial(kernel, ny, nx), out_shape=jax.ShapeDtyp...]
    all_to_all x5 -> x0, blocking collectives: 68.8 us -> none  [the longest x1 23.8 us: local(): lax.all_to_all(heads_out, 'tp', split_axis=1, concat_axis=0, tiled=True)]
    all_gather x1 -> x0, waiting for transfers between devices: 35.6 us -> none  [stacked_from(): blocks = lax.all_gather(blocks, axes[k], axis=0, tiled=True)]
    all_to_all x3 -> x0, starting transfers between devices: 29.3 us -> none  [the longest x1 11.8 us: local(): lax.all_to_all(summed.astype(jnp.bfloat16), EP, split_axis=0, concat_axis...]
    all_to_all x3 -> x0, waiting for transfers between devices: 22.8 us -> none  [the longest x1 13.3 us: local(): lax.all_to_all(outputs.reshape(ep_count, item_count, width), EP, split_ax...]
    all_gather x1 -> x0, blocking collectives: 20.8 us -> none  [stacked_from(): blocks = lax.all_gather(blocks, axes[k], axis=0, tiled=True)]
    dot_general x14 -> x0, matrix products: 13.5 us -> none  [the longest x2 2.87 us: swiglu(): jnp.dot(inner_rows, down_w, preferred_element_type=jnp.float32)]
    convert_element_type x9 -> x0, other arithmetic: 3.04 us -> none  [the longest x1 0.76 us: local(): latent_new.astype(jnp.float32)[:, None, :]]
  transfers between devices with their start and end apart: 4 -> 0, of which waited for: 3 -> 0; matrix products, arithmetic and copies ran while one was open for 2% -> 0% of each run, Pallas kernels for 0% -> 0%
where the time goes in v1:
time: 81.4 us; the launch traced here: 81.3 us
  Pallas kernels  79.9 us (98%)
  local copies, waits for them, and re-layouts  1.38 us (2%)
    pallas_call x1, Pallas kernels, local(): pl.pallas_call(functools.partial(kernel, ny, nx), out_shape=jax.ShapeDtyp...  79.9 us

profile of v1, /device:TPU:513, one launch (start us, length us, event | category | flops | bytes accessed | tf_op | source)
XLA Modules:
  0.0 81.3 jit_solution(16859119086159381707)
XLA Ops:
  0.0 79.9 %layer.1 = bf16[8,2048]{1,0:T(8,128)(2,1)} custom-call(s32[8]{0:T(128)} %lens.1, bf16[8,2048]{1,0:T(8,128)(2,1)} %hid_hbm.1, bf16[8,16,64]{2,1,0:T(8,128)(2,1)} %qn_hbm.1, bf16[8,16,32]{2,1,0:T(8,128)(2,1)} %qr_hbm.1, bf16[8,256]{1,0:T(8,128)(2,1)} %nl_hbm.1, bf16[8,32]{1,0:T(8,128)(2,1)} %nr_hbm.1, bf16[8,1024,256]{2,1,0:T(8,128)(2,1)} %cl_hbm.1, ...), custom_call_target="tpu_custom_call" | custom-call | tf_op jit(solution)/shard_map/layer/pallas_call | solution.py:558
  79.9 1.4 %copy.24 = bf16[8,2048]{1,0:T(8,128)(2,1)} copy(bf16[8,2048]{1,0:T(8,128)(2,1)} %layer.1) | data formatting | bytes 65536

commit v2 on v1

--- a/solution.py
+++ b/solution.py
@@ -45,10 +45,21 @@
     return sorted(range(1, n), key=lambda d: (-min(d, n - d), d))
 
 
+def near_offsets(n):
+    return [d for d in far_first(n) if n < 8 or min(d, n - d) <= 2]
+
+
+def weight_block(ref, part):
+    if part is None:
+        return ref
+    half = ref.shape[1] // 2
+    return ref.at[:, pl.ds(part * half, half)]
+
+
 def kernel(
     ny,
     nx,
-    lens,
+    lens_hbm,
     hid_hbm,
     qn_hbm,
     qr_hbm,
@@ -71,6 +82,7 @@
     su_hbm,
     sd_hbm,
     out_ref,
+    lens,
     hid,
     qn,
     qr,
@@ -111,6 +123,7 @@
     part,
     pb,
     shr,
+    ready,
     lsem,
     csem,
     hsend,
@@ -119,6 +132,7 @@
     wrecv,
     w2send,
     w2recv,
+    w3send,
     asend,
     arecv,
     msend,
@@ -151,22 +165,6 @@
             src_ref=src, dst_ref=dst, send_sem=ssem, recv_sem=rsem, device_id=dev(*where), device_id_type=MESH
         )
 
-    barrier = pltpu.get_barrier_semaphore()
-
-    def greet(ty, tx, tt):
-        pl.semaphore_signal(barrier, inc=1, device_id=dev(ty, tx, tt), device_id_type=MESH)
-
-    def greet_ep(k, _):
-        k = lax.rem(me + k, n_ep)
-        greet(k // nx, lax.rem(k, nx), t)
-        return 0
-
-    greet(y, x, u)
-    lax.fori_loop(1, n_ep, greet_ep, 0)
-    for d in range(1, ny):
-        greet(lax.rem(y + d, ny), x, u)
-    peers = 1 + (n_ep - 1) + (ny - 1)
-
     small = [
         (qn_hbm, qn),
         (ak_hbm, ak),
@@ -174,9 +172,9 @@
         (nl_hbm, nl),
         (nr_hbm, nr),
         (vu_hbm, vu),
-        (wt_hbm, wtb.at[x, t]),
         (routes_hbm, routes),
         (hid_hbm, hid.at[t]),
+        (wt_hbm, wtb.at[x, t]),
         (gmix_hbm, gmix),
         (gin_hbm, gin),
         (gout_hbm, gout),
@@ -187,6 +185,7 @@
         (eg_hbm, eg),
         (eu_hbm, eu),
         (ed_hbm, ed),
+        (lens_hbm, lens),
     ]
     loads = [pltpu.make_async_copy(a, b, lsem.at[i]) for i, (a, b) in enumerate(small)]
     cache = []
@@ -197,20 +196,37 @@
                 pltpu.make_async_copy(cr_hbm.at[s], cr.at[s], csem.at[1, s]),
             )
         )
-    for i in range(5):
+    for i in (0, 1):
         loads[i].start()
-    for a, b in cache:
+    for a, b in cache[:1]:
         a.start()
         b.start()
-    for i in range(5, len(loads)):
+    for i in (8, len(loads) - 1, 2, 3, 4):
         loads[i].start()
+    for a, b in cache[1:]:
+        a.start()
+        b.start()
+    loads[5].start()
+
+    barrier = pltpu.get_barrier_semaphore()
+
+    def greet(ty, tx, tt):
+        pl.semaphore_signal(barrier, inc=1, device_id=dev(ty, tx, tt), device_id_type=MESH)
+
+    for d in range(1, nx):
+        greet(y, lax.rem(x + d, nx), t)
+    for d in range(1, ny):
+        for tt in (t, u):
+            greet(lax.rem(y + d, ny), x, tt)
+    greet(y, x, u)
+    peers = (nx - 1) + 2 * (ny - 1) + 1
 
     loads[0].wait()
     loads[1].wait()
     q32[...] = qn[...].astype(F32)
     for h in range(heads):
         ql[:, h, :] = mm(q32[:, h, :].astype(BF16), ak[h])
-    for i in (2, 3, 4):
+    for i in (2, 3, 4, len(loads) - 1):
         loads[i].wait()
     rope = nr.shape[1]
     half = rope // 2
@@ -230,7 +246,20 @@
 
     ctx = cl.shape[1]
     key_at = iota((heads, ctx), 1)
+    w_out = []
     for s in range(seqs):
+        if s == seqs // 2:
+            for i in list(range(6, 8)) + list(range(9, len(loads) - 1)):
+                loads[i].start()
+        if s == 1:
+            loads[8].wait()
+            pl.semaphore_wait(barrier, peers)
+            for d in range(1, nx):
+                pl.semaphore_signal(ready, inc=1, device_id=dev(y, lax.rem(x + d, nx), t), device_id_type=MESH)
+            for d in near_offsets(nx):
+                c = remote(wtb.at[x, t], wtb.at[x, t], wsend.at[d], wrecv.at[d], (y, lax.rem(x + d, nx), t))
+                c.start()
+                w_out.append(c)
         q_s = ql[s].astype(BF16)
         r_s = qr[s]
         pe_s = (r_s.astype(F32) * cos[s : s + 1, :] + mm(r_s, swap) * sin[s : s + 1, :]).astype(BF16)
@@ -260,26 +289,46 @@
     for h in range(heads):
         abuf[y, :, h * vh : (h + 1) * vh] = mm(lo[:, h, :].astype(BF16), vut[h]).astype(BF16)
 
-    pl.semaphore_wait(barrier, peers)
     a_out = []
     for d in far_first(ny):
         c = remote(abuf.at[y], abuf.at[y], asend.at[d], arecv.at[d], (lax.rem(y + d, ny), x, t))
         c.start()
         a_out.append(c)
-    loads[6].wait()
-    w_out = []
-    for d in far_first(nx):
-        c = remote(wtb.at[x, t], wtb.at[x, t], wsend.at[d], wrecv.at[d], (y, lax.rem(x + d, nx), t))
+    w2_out = []
+
+    def weight_came(d, part):
+        block = weight_block(wtb.at[lax.rem(x + nx - d, nx), t], part)
+        remote(block, block, wsend.at[d], wrecv.at[d], (y, x, u)).wait_recv()
+
+    def pass_on(d, to, part, at):
+        block = weight_block(wtb.at[lax.rem(x + nx - d, nx), t], part)
+        c = remote(block, block, w3send.at[at], wrecv.at[at], (y, lax.rem(x + to, nx), t))
         c.start()
         w_out.append(c)
-    loads[8].wait()
+
+    def to_partner(d, part, at):
+        block = weight_block(wtb.at[lax.rem(x + nx - d, nx), t], part)
+        c = remote(block, block, w2send.at[at], w2recv.at[at], (y, x, u))
+        c.start()
+        w2_out.append(c)
+
+    near = near_offsets(nx)
+    if len(near) < nx - 1:
+        weight_came(2, None)
+        pass_on(2, 2, 0, 4)
+        pass_on(2, 1, None, 3)
+        weight_came(nx - 2, None)
+        pass_on(nx - 2, nx - 2, 1, 8)
+        pass_on(nx - 2, nx - 1, None, nx - 3)
+        to_partner(2, None, 2)
+        to_partner(nx - 2, None, nx - 2)
+    to_partner(0, None, 0)
+    loads[7].wait()
     h_out = remote(hid.at[t], hid.at[t], hsend, hrecv, (y, x, u))
     h_out.start()
-    w2_out = [remote(wtb.at[x, t], wtb.at[x, t], w2send.at[0], w2recv.at[0], (y, x, u))]
-    w2_out[0].start()
 
     tokens = 2 * seqs
-    loads[7].wait()
+    loads[6].wait()
     routes_t = routes[...]
     top_k = routes_t.shape[0]
     expert_at = iota((experts, tokens), 0)
@@ -298,18 +347,26 @@
     b0 = mm(pick, rep(first).astype(BF16))
     b1 = mm(pick, rep(second).astype(BF16))
     disp[...] = jnp.where(r_q == c_q, jnp.where(r_cap == 0, b0, b1), 0.0).astype(BF16)
-    pr, pc = iota((rows_r, rows_r), 0), iota((rows_r, rows_r), 1)
-    k = pr % rows_x
-    perm[...] = (pc == (k // CAP) * (Q * CAP) + (pr // rows_x) * CAP + k % CAP).astype(BF16)
-    k = pc % rows_x
-    permt[...] = (pr == (k // CAP) * (Q * CAP) + (pc // rows_x) * CAP + k % CAP).astype(BF16)
-
-    for i, d in enumerate(far_first(nx)[::-1]):
-        sx = lax.rem(x + nx - d, nx)
-        remote(wtb.at[sx, t], wtb.at[sx, t], wsend.at[d], wrecv.at[d], (y, x, u)).wait_recv()
-        c = remote(wtb.at[sx, t], wtb.at[sx, t], w2send.at[d], w2recv.at[d], (y, x, u))
-        c.start()
-        w2_out.append(c)
+    rows_c = perm.shape[0]
+    of_q = rows_c // Q
+    pr, pc = iota((rows_c, rows_c), 0), iota((rows_c, rows_c), 1)
+    k = pr % of_q
+    perm[...] = (pc == (k // CAP) * (Q * CAP) + (pr // of_q) * CAP + k % CAP).astype(BF16)
+    k = pc % of_q
+    permt[...] = (pr == (k // CAP) * (Q * CAP) + (pc // of_q) * CAP + k % CAP).astype(BF16)
+
+    if len(near) < nx - 1:
+        for d in (1, nx - 1, 3, nx - 3):
+            weight_came(d, None)
+            to_partner(d, None, d)
+        for half_at, at in ((0, 4), (1, 8)):
+            block = weight_block(wtb.at[lax.rem(x + nx - 4, nx), t], half_at)
+            remote(block, block, w3send.at[at], wrecv.at[at], (y, x, u)).wait_recv()
+            to_partner(4, half_at, at)
+    else:
+        for d in near:
+            weight_came(d, None)
+            to_partner(d, None, d)
     for d in far_first(ny):
         remote(abuf.at[y], abuf.at[y], asend.at[d], arecv.at[d], (y, x, u)).wait_recv()
     for c in w2_out:
@@ -329,7 +386,7 @@
     c.start()
     m_out.append(c)
     mb[y, t] = mo[y]
-    for i in range(9, len(loads)):
+    for i in range(9, len(loads) - 1):
         loads[i].wait()
     h_out.wait_recv()
     for d in far_first(ny):
@@ -349,23 +406,36 @@
     ffs[...] = ffn.astype(F32).reshape(2, seqs, width)
 
     stack = jnp.concatenate([ffn[:, i * qw : (i + 1) * qw] for i in range(Q)], axis=0)
+    pl.semaphore_wait(ready, nx - 1)
+    chunks = [
+        sorted(
+            [(dy, (dy + k) % nx) for k in (2 * c, 2 * c + 1) for dy in range(ny)],
+            key=lambda o: (-(min(o[0], ny - o[0]) + min(o[1], nx - o[1])), (o[0] + o[1]) % 2, o),
+        )
+        for c in range(nx // 2)
+    ]
+    chunks = chunks[1:] + chunks[:1]
+
+    def at(dy, dx):
+        return lax.rem(y + dy + ny, ny), lax.rem(x + dx + nx, nx)
+
+    def post(src, dst, ssem, rsem, ty, tx):
+        remote(src.at[ty * nx + tx], dst.at[me], ssem, rsem, (ty, tx, t)).start()
+
+    def came(buf, rsem, c):
+        some = buf.at[pl.ds(0, len(chunks[c]) - ((0, 0) in chunks[c]))]
+        pltpu.make_async_copy(some, some, rsem.at[c]).wait()
+
+    def left(buf, ssem):
+        some = buf.at[pl.ds(0, n_ep - 1)]
+        pltpu.make_async_copy(some, some, ssem).wait()
+
     sb[...] = mm(disp[...], stack).reshape(n_ep, Q * CAP, qw).astype(BF16)
-    offsets = sorted(
-        [(dy, dx) for dy in range(ny) for dx in range(nx) if (dy, dx) != (0, 0)],
-        key=lambda o: (-(min(o[0], ny - o[0]) + min(o[1], nx - o[1])), (o[0] + o[1]) % 2, o),
-    )
-
-    def spread(src, dst, ssem, rsem):
-        for dy, dx in offsets:
-            ty, tx = lax.rem(y + dy, ny), lax.rem(x + dx, nx)
-            remote(src.at[ty * nx + tx], dst.at[me], ssem, rsem, (ty, tx, t)).start()
-        dst[me] = src[me]
-
-    def arrived(buf, sem):
-        some = buf.at[pl.ds(0, n_ep - 1)]
-        pltpu.make_async_copy(some, some, sem).wait()
-
-    spread(sb, rb, dsend, drecv)
+    for c, chunk in enumerate(chunks):
+        for dy, dx in chunk:
+            if (dy, dx) != (0, 0):
+                post(sb, rb, dsend, drecv.at[c], *at(dy, dx))
+    rb[me] = sb[me]
 
     own = ffs[t].astype(BF16)
     s_gate = mm(own, sg[...])
@@ -395,20 +465,29 @@
     g_hi = combine_of(lambda v: v.astype(BF16))
     g_lo = combine_of(lambda v: (v - v.astype(BF16).astype(F32)).astype(BF16))
 
-    arrived(rb, drecv)
-    turned = mm(perm[...], rb[...].reshape(rows_r, qw)).astype(BF16)
-    gate = jnp.zeros((rows_x, eg.shape[1]), F32)
-    up = jnp.zeros((rows_x, eg.shape[1]), F32)
-    for i in range(Q):
-        piece = turned[i * rows_x : (i + 1) * rows_x, :]
-        gate = gate + mm(piece, eg[i * qw : (i + 1) * qw, :])
-        up = up + mm(piece, eu[i * qw : (i + 1) * qw, :])
-    e_hid = (gate / (1.0 + jnp.exp(-gate)) * up).astype(BF16)
-    e_out = jnp.concatenate([mm(e_hid, ed[:, i * qw : (i + 1) * qw]).astype(BF16) for i in range(Q)], axis=0)
-    sb2[...] = mm(permt[...], e_out).reshape(n_ep, Q * CAP, qw).astype(BF16)
-    spread(sb2, cb, csend, crecv)
-
-    arrived(cb, crecv)
+    for c, chunk in enumerate(chunks):
+        sources = [at(-dy, -dx) for dy, dx in chunk]
+        came(rb, drecv, c)
+        got = [rb[sy * nx + sx] for sy, sx in sources]
+        turned = mm(perm[...], jnp.concatenate(got, axis=0)).astype(BF16)
+        gate = jnp.zeros((of_q, eg.shape[1]), F32)
+        up = jnp.zeros((of_q, eg.shape[1]), F32)
+        for j in range(Q):
+            piece = turned[j * of_q : (j + 1) * of_q, :]
+            gate = gate + mm(piece, eg[j * qw : (j + 1) * qw, :])
+            up = up + mm(piece, eu[j * qw : (j + 1) * qw, :])
+        e_hid = (gate / (1.0 + jnp.exp(-gate)) * up).astype(BF16)
+        e_out = jnp.concatenate([mm(e_hid, ed[:, j * qw : (j + 1) * qw]).astype(BF16) for j in range(Q)], axis=0)
+        back = mm(permt[...], e_out).astype(BF16)
+        for j, (sy, sx) in enumerate(sources):
+            sb2[sy * nx + sx] = back[j * Q * CAP : (j + 1) * Q * CAP, :]
+        for (dy, dx), (sy, sx) in zip(chunk, sources):
+            if (dy, dx) != (0, 0):
+                post(sb2, cb, csend, crecv.at[c], sy, sx)
+    cb[me] = sb2[me]
+
+    for c in range(len(chunks)):
+        came(cb, crecv, c)
     c_all = cb[...].reshape(rows_r, qw)
     routed = mm(g_hi, c_all) + mm(g_lo, c_all)
     part[...] = routed.reshape(2, Q * seqs, qw)
@@ -424,8 +503,8 @@
 
     for c in a_out + w_out + w2_out + m_out + [h_out, p_out]:
         c.wait_send()
-    arrived(sb, dsend)
-    arrived(sb2, csend)
+    left(sb, dsend)
+    left(sb2, csend)
 
 
 def local(
@@ -495,6 +574,7 @@
         return v(args[i].shape, args[i].dtype)
 
     scratch = [
+        pltpu.SMEM(lengths.shape, lengths.dtype),
         v((2, seqs, width), BF16),
         like(2),
         like(3),
@@ -525,8 +605,8 @@
         v((ny, 2, seqs, nx * 2 * col), BF16),
         v((2, seqs, width), F32),
         v((2, seqs, width), F32),
-        v((rows_r, rows_r), BF16),
-        v((rows_r, rows_r), BF16),
+        v((2 * ny * Q * CAP, 2 * ny * Q * CAP), BF16),
+        v((2 * ny * Q * CAP, 2 * ny * Q * CAP), BF16),
         v((rows_r, Q * tokens), BF16),
         v((n_ep, Q * CAP, qw), BF16),
         v((n_ep, Q * CAP, qw), BF16),
@@ -535,22 +615,24 @@
         v((2, Q * seqs, qw), F32),
         v((Q * seqs, qw), F32),
         v((Q * seqs, qw), F32),
-        dma((19,)),
+        pltpu.SemaphoreType.REGULAR,
+        dma((20,)),
         dma((2, seqs)),
         dma,
         dma,
         dma((nx,)),
-        dma((nx,)),
-        dma((nx,)),
-        dma((nx,)),
+        dma((nx + 1,)),
+        dma((nx + 1,)),
+        dma((nx + 1,)),
+        dma((nx + 1,)),
         dma((ny,)),
         dma((ny,)),
         dma((2, ny)),
         dma((2, ny)),
         dma,
+        dma((ny,)),
         dma,
-        dma,
-        dma,
+        dma((ny,)),
         dma,
         dma,
     ]
@@ -558,7 +640,7 @@
     return pl.pallas_call(
         functools.partial(kernel, ny, nx),
         out_shape=jax.ShapeDtypeStruct((seqs, width), BF16),
-        in_specs=[pl.BlockSpec(memory_space=pltpu.SMEM)] + [hbm] * (len(args) - 1),
+        in_specs=[hbm] * len(args),
         out_specs=pl.BlockSpec(memory_space=pltpu.VMEM),
         scratch_shapes=scratch,
         compiler_params=pltpu.CompilerParams(

time: 81.4 us -> 75.1 us (0.923)
  Pallas kernels: 79.9 us -> 73.4 us
    pallas_call x1, Pallas kernels: 79.9 us -> 73.4 us  [local(): pl.pallas_call(functools.partial(kernel, ny, nx), out_shape=jax.ShapeDtyp...]
where the time goes in v2:
time: 75.1 us; the launch traced here: 74.7 us
  Pallas kernels  73.4 us (98%)
  local copies, waits for them, and re-layouts  1.38 us (2%)
    pallas_call x1, Pallas kernels, local(): pl.pallas_call(functools.partial(kernel, ny, nx), out_shape=jax.ShapeDtyp...  73.4 us

profile of v2, /device:TPU:513, one launch (start us, length us, event | category | flops | bytes accessed | tf_op | source)
XLA Modules:
  0.0 74.7 jit_solution(14404261985978914030)
XLA Ops:
  0.0 73.4 %layer.1 = bf16[8,2048]{1,0:T(8,128)(2,1)} custom-call(s32[8]{0:T(128)} %lens_hbm.1, bf16[8,2048]{1,0:T(8,128)(2,1)} %hid_hbm.1, bf16[8,16,64]{2,1,0:T(8,128)(2,1)} %qn_hbm.1, bf16[8,16,32]{2,1,0:T(8,128)(2,1)} %qr_hbm.1, bf16[8,256]{1,0:T(8,128)(2,1)} %nl_hbm.1, bf16[8,32]{1,0:T(8,128)(2,1)} %nr_hbm.1, bf16[8,1024,256]{2,1,0:T(8,128)(2,1)} %cl_hbm.1, ...), custom_call_target="tpu_custom_call" | custom-call | tf_op jit(solution)/shard_map/layer/pallas_call | solution.py:640
  73.4 1.4 %copy.24 = bf16[8,2048]{1,0:T(8,128)(2,1)} copy(bf16[8,2048]{1,0:T(8,128)(2,1)} %layer.1) | data formatting | bytes 65536

commit v3 on v2

--- a/solution.py
+++ b/solution.py
@@ -198,15 +198,12 @@
         )
     for i in (0, 1):
         loads[i].start()
-    for a, b in cache[:1]:
+    for i in (8, len(loads) - 1, 2, 3, 4):
+        loads[i].start()
+    ahead = min(3, seqs // 2)
+    for a, b in cache[: 2 * ahead]:
         a.start()
         b.start()
-    for i in (8, len(loads) - 1, 2, 3, 4):
-        loads[i].start()
-    for a, b in cache[1:]:
-        a.start()
-        b.start()
-    loads[5].start()
 
     barrier = pltpu.get_barrier_semaphore()
 
@@ -247,19 +244,8 @@
     ctx = cl.shape[1]
     key_at = iota((heads, ctx), 1)
     w_out = []
-    for s in range(seqs):
-        if s == seqs // 2:
-            for i in list(range(6, 8)) + list(range(9, len(loads) - 1)):
-                loads[i].start()
-        if s == 1:
-            loads[8].wait()
-            pl.semaphore_wait(barrier, peers)
-            for d in range(1, nx):
-                pl.semaphore_signal(ready, inc=1, device_id=dev(y, lax.rem(x + d, nx), t), device_id_type=MESH)
-            for d in near_offsets(nx):
-                c = remote(wtb.at[x, t], wtb.at[x, t], wsend.at[d], wrecv.at[d], (y, lax.rem(x + d, nx), t))
-                c.start()
-                w_out.append(c)
+
+    def scores(s):
         q_s = ql[s].astype(BF16)
         r_s = qr[s]
         pe_s = (r_s.astype(F32) * cos[s : s + 1, :] + mm(r_s, swap) * sin[s : s + 1, :]).astype(BF16)
@@ -267,17 +253,47 @@
             jnp.sum(q_s.astype(F32) * lat_new[s : s + 1, :], axis=-1, keepdims=True)
             + jnp.sum(pe_s.astype(F32) * key_new[s : s + 1, :], axis=-1, keepdims=True)
         ) * scale
-        cache[s][0].wait()
-        cache[s][1].wait()
-        k_s = cl[s]
-        sc = (mm_nt(q_s, k_s) + mm(pe_s, cr[s])) * scale
-        sc = jnp.where(key_at < lens[s], sc, MASKED)
+        sc = (mm_nt(q_s, cl[s]) + mm(pe_s, cr[s])) * scale
+        return s, jnp.where(key_at < lens[s], sc, MASKED), s_new
+
+    def attend(s, sc, s_new):
         top = jnp.maximum(jnp.max(sc, axis=-1, keepdims=True), s_new)
         p = jnp.exp(sc - top)
         p_new = jnp.exp(s_new - top)
         total = jnp.sum(p, axis=-1, keepdims=True) + p_new
-        acc = mm(p.astype(BF16), k_s) + p_new.astype(BF16).astype(F32) * lat_new[s : s + 1, :]
+        acc = mm(p.astype(BF16), cl[s]) + p_new.astype(BF16).astype(F32) * lat_new[s : s + 1, :]
         lo[s] = acc / total
+
+    pairs = seqs // 2
+    scored = []
+    for p in range(pairs + 1):
+        if p == 1:
+            loads[8].wait()
+            pl.semaphore_wait(barrier, peers)
+            for d in near_offsets(nx):
+                c = remote(wtb.at[x, t], wtb.at[x, t], wsend.at[d], wrecv.at[d], (y, lax.rem(x + d, nx), t))
+                c.start()
+                w_out.append(c)
+            for d in range(1, nx):
+                pl.semaphore_signal(ready, inc=1, device_id=dev(y, lax.rem(x + d, nx), t), device_id_type=MESH)
+        if p == 2:
+            for i in list(range(6, 8)) + list(range(9, len(loads) - 1)):
+                loads[i].start()
+        before = scored
+        scored = []
+        if p < pairs:
+            for s in (2 * p, 2 * p + 1):
+                cache[s][0].wait()
+                cache[s][1].wait()
+            if p + ahead < pairs:
+                for s in (2 * (p + ahead), 2 * (p + ahead) + 1):
+                    cache[s][0].start()
+                    cache[s][1].start()
+            elif p + ahead == pairs:
+                loads[5].start()
+            scored = [scores(s) for s in (2 * p, 2 * p + 1)]
+        for one in before:
+            attend(*one)
 
     lat = vut.shape[1]
     pv = (iota((256, 256), 1) == (iota((256, 256), 0) % 16) * heads + iota((256, 256), 0) // 16).astype(BF16)

time: 75.1 us -> 71.3 us (0.949)
  Pallas kernels: 73.4 us -> 69.3 us
    pallas_call x1, Pallas kernels: 73.4 us -> 69.3 us  [local(): pl.pallas_call(functools.partial(kernel, ny, nx), out_shape=jax.ShapeDtyp...]
where the time goes in v3:
time: 71.3 us; the launch traced here: 70.7 us
  Pallas kernels  69.3 us (97%)
  local copies, waits for them, and re-layouts  1.38 us (2%)
    pallas_call x1, Pallas kernels, local(): pl.pallas_call(functools.partial(kernel, ny, nx), out_shape=jax.ShapeDtyp...  69.3 us

profile of v3, /device:TPU:513, one launch (start us, length us, event | category | flops | bytes accessed | tf_op | source)
XLA Modules:
  0.0 70.7 jit_solution(11678207854399421687)
XLA Ops:
  0.0 69.3 %layer.1 = bf16[8,2048]{1,0:T(8,128)(2,1)} custom-call(s32[8]{0:T(128)} %lens_hbm.1, bf16[8,2048]{1,0:T(8,128)(2,1)} %hid_hbm.1, bf16[8,16,64]{2,1,0:T(8,128)(2,1)} %qn_hbm.1, bf16[8,16,32]{2,1,0:T(8,128)(2,1)} %qr_hbm.1, bf16[8,256]{1,0:T(8,128)(2,1)} %nl_hbm.1, bf16[8,32]{1,0:T(8,128)(2,1)} %nr_hbm.1, bf16[8,1024,256]{2,1,0:T(8,128)(2,1)} %cl_hbm.1, ...), custom_call_target="tpu_custom_call" | custom-call | tf_op jit(solution)/shard_map/layer/pallas_call | solution.py:656
  69.4 1.4 %copy.24 = bf16[8,2048]{1,0:T(8,128)(2,1)} copy(bf16[8,2048]{1,0:T(8,128)(2,1)} %layer.1) | data formatting | bytes 65536

commit v4 on v3

--- a/solution.py
+++ b/solution.py
@@ -267,7 +267,7 @@
     pairs = seqs // 2
     scored = []
     for p in range(pairs + 1):
-        if p == 1:
+        if p == 2:
             loads[8].wait()
             pl.semaphore_wait(barrier, peers)
             for d in near_offsets(nx):
@@ -655,7 +655,7 @@
     hbm = pl.BlockSpec(memory_space=pltpu.HBM)
     return pl.pallas_call(
         functools.partial(kernel, ny, nx),
-        out_shape=jax.ShapeDtypeStruct((seqs, width), BF16),
+        out_shape=pltpu.VMEM((seqs, width), BF16),
         in_specs=[hbm] * len(args),
         out_specs=pl.BlockSpec(memory_space=pltpu.VMEM),
         scratch_shapes=scratch,

time: 71.3 us -> 69.6 us (0.976)
  local copies, waits for them, and re-layouts: 1.38 us -> 0.62 us
    unnamed x1, local copies, waits for them, and re-layouts: 1.38 us -> 0.62 us
where the time goes in v4:
time: 69.6 us; the launch traced here: 69.5 us
  Pallas kernels  68.8 us (99%)
    pallas_call x1, Pallas kernels, local(): pl.pallas_call(functools.partial(kernel, ny, nx), out_shape=pltpu.VMEM((s...  68.8 us

profile of v4, /device:TPU:513, one launch (start us, length us, event | category | flops | bytes accessed | tf_op | source)
XLA Modules:
  0.0 69.5 jit_solution(11712689411960219445)
XLA Ops:
  0.0 68.8 %layer.1 = bf16[8,2048]{1,0:T(8,128)(2,1)S(1)} custom-call(s32[8]{0:T(128)} %lens_hbm.1, bf16[8,2048]{1,0:T(8,128)(2,1)} %hid_hbm.1, bf16[8,16,64]{2,1,0:T(8,128)(2,1)} %qn_hbm.1, bf16[8,16,32]{2,1,0:T(8,128)(2,1)} %qr_hbm.1, bf16[8,256]{1,0:T(8,128)(2,1)} %nl_hbm.1, bf16[8,32]{1,0:T(8,128)(2,1)} %nr_hbm.1, bf16[8,1024,256]{2,1,0:T(8,128)(2,1)} %cl_hbm.1, ...), custom_call_target="tpu_custom_call" | custom-call | tf_op jit(solution)/shard_map/layer/pallas_call | solution.py:656
  68.9 0.6 copy.24

commit v5 on v4

--- a/solution.py
+++ b/solution.py
@@ -505,7 +505,8 @@
     for c in range(len(chunks)):
         came(cb, crecv, c)
     c_all = cb[...].reshape(rows_r, qw)
-    routed = mm(g_hi, c_all) + mm(g_lo, c_all)
+    both = mm(jnp.concatenate([g_hi, g_lo], axis=0), c_all)
+    routed = both[: Q * tokens, :] + both[Q * tokens :, :]
     part[...] = routed.reshape(2, Q * seqs, qw)
     p_out = remote(part.at[u], pb, psend, precv, (y, x, u))
     p_out.start()

time: 69.6 us -> 69.5 us (level)
  no operation moved by 1% of the time
where the time goes in v5:
time: 69.5 us; the launch traced here: 69.4 us
  Pallas kernels  68.8 us (99%)
    pallas_call x1, Pallas kernels, local(): pl.pallas_call(functools.partial(kernel, ny, nx), out_shape=pltpu.VMEM((s...  68.8 us

profile of v5, /device:TPU:513, one launch (start us, length us, event | category | flops | bytes accessed | tf_op | source)
XLA Modules:
  0.0 69.4 jit_solution(13901924480335035913)
XLA Ops:
  0.0 68.8 %layer.1 = bf16[8,2048]{1,0:T(8,128)(2,1)S(1)} custom-call(s32[8]{0:T(128)} %lens_hbm.1, bf16[8,2048]{1,0:T(8,128)(2,1)} %hid_hbm.1, bf16[8,16,64]{2,1,0:T(8,128)(2,1)} %qn_hbm.1, bf16[8,16,32]{2,1,0:T(8,128)(2,1)} %qr_hbm.1, bf16[8,256]{1,0:T(8,128)(2,1)} %nl_hbm.1, bf16[8,32]{1,0:T(8,128)(2,1)} %nr_hbm.1, bf16[8,1024,256]{2,1,0:T(8,128)(2,1)} %cl_hbm.1, ...), custom_call_target="tpu_custom_call" | custom-call | tf_op jit(solution)/shard_map/layer/pallas_call | solution.py:657
  68.8 0.6 copy.24
